TPU v7x, 32 devices: a whole 2x2x4 slice. The times are simulated.
32 devices in a mesh: st: 16 (over z, y, x), tp: 2 (over core).
Axes of the slice: x: 2, y: 2, z: 4, core: 2. Of those that a mesh axis runs over, the one named last changes fastest.
Arguments:
- hidden: bfloat16 [8192, 2048], P('st'), may hold values from -24 to 24
- passage_store: bfloat16 [512, 64, 2048], P('st'), may hold values from -6 to 6
- passage_ids: int32 [128, 4], P('st'), may hold values from 0 to 511, as said below
- query_weight: bfloat16 [2048, 512], P(None, 'tp'), may hold values from -0.125 to 0.125
- gate_weight: bfloat16 [2048, 512], P(None, 'tp'), may hold values from -0.125 to 0.125
- key_weight: bfloat16 [2048, 512], P(None, 'tp'), may hold values from -0.125 to 0.125
- value_weight: bfloat16 [2048, 512], P(None, 'tp'), may hold values from -0.125 to 0.125
- output_grad: bfloat16 [8192, 512], P('st', 'tp'), may hold values from -6 to 6
Outputs:
- grad_hidden: bfloat16 [8192, 2048], P(('st', 'tp'))
- grad_store: bfloat16 [512, 64, 2048], P(('st', 'tp'))
- grad_value_weight: float32 [2048, 512], P(None, 'tp')
Inputs may be any that keep to these rules, and one draw needn't show every extreme that they name: `passage_ids`: passage p is held at st index p // 32. The 32 ids of one index of st (its 8 blocks) are distinct; at most 4 of them name passages of one owner, and on every index some owner is named exactly 4 times. Every index reads at least one passage of the owner before it, of the owner after it and of the owner half the axis away.
All inputs are finite; a program needn't handle non-finite values.
Results may differ from a plain program's by a relative error of at most 0.012.
The roundings to bfloat16 on the way count: a program that leaves them out, or rounds other values in their place, can miss the bound.
Values may be sent and summed in bfloat16 or wider, within the bound.
A program may use at most 128 MiB of HBM per device.

v0:
```python
import jax
import jax.numpy as jnp
from jax import lax
from jax.sharding import PartitionSpec as P

HEAD_DIM = 256


def body(
    hidden,
    passage_store,
    passage_ids,
    query_weight,
    gate_weight,
    key_weight,
    value_weight,
    output_grad,
):
    owner_count = lax.axis_size("st")
    own_index = lax.axis_index("st")
    held_count = passage_store.shape[0]
    span_rows = passage_store.shape[1]
    model_width = passage_store.shape[2]
    block_count = passage_ids.shape[0]
    per_block = passage_ids.shape[1]
    requests = block_count * per_block
    capacity = max(1, 2 * requests // owner_count)
    local_width = query_weight.shape[1]
    local_heads = local_width // HEAD_DIM
    tokens_here = hidden.shape[0]
    block_rows = tokens_here // block_count
    all_ids = lax.all_gather(passage_ids, "st", axis=0, tiled=True).reshape(owner_count, requests)
    owner_of = all_ids // held_count
    local_index = all_ids % held_count
    positions = jnp.arange(requests, dtype=jnp.int32)
    earlier = positions[None, :] < positions[:, None]
    matching = owner_of[:, :, None] == owner_of[:, None, :]
    slot_rank = jnp.sum(matching & earlier[None], axis=2)
    slot_iota = jnp.arange(capacity, dtype=jnp.int32)
    placed = (owner_of == own_index)[:, :, None] & (
        slot_rank[:, :, None] == slot_iota[None, None, :]
    )
    slot_table = jnp.sum(jnp.where(placed, local_index[:, :, None], 0), axis=1)
    filled = jnp.any(placed, axis=1)
    my_owner = lax.dynamic_index_in_dim(owner_of, own_index, 0, keepdims=False)
    my_rank = lax.dynamic_index_in_dim(slot_rank, own_index, 0, keepdims=False)
    slot_flat = my_owner * capacity + my_rank
    store_rows = passage_store.reshape(held_count * span_rows, model_width)
    keys_here = (
        jnp.dot(store_rows, key_weight, preferred_element_type=jnp.float32)
        .astype(jnp.bfloat16)
        .reshape(held_count, span_rows, local_width)
    )
    values_here = (
        jnp.dot(store_rows, value_weight, preferred_element_type=jnp.float32)
        .astype(jnp.bfloat16)
        .reshape(held_count, span_rows, local_width)
    )
    came_keys, came_values = (
        lax.all_to_all(keys_here[slot_table], "st", split_axis=0, concat_axis=0, tiled=True),
        lax.all_to_all(values_here[slot_table], "st", split_axis=0, concat_axis=0, tiled=True),
    )
    got_keys = came_keys.reshape(owner_count * capacity, span_rows, local_width)[slot_flat]
    got_values = came_values.reshape(owner_count * capacity, span_rows, local_width)[slot_flat]
    key_heads = got_keys.reshape(block_count, per_block * span_rows, local_heads, HEAD_DIM)
    value_heads = got_values.reshape(block_count, per_block * span_rows, local_heads, HEAD_DIM)
    queries = jnp.dot(hidden, query_weight, preferred_element_type=jnp.float32).astype(jnp.bfloat16)
    gates = jnp.dot(hidden, gate_weight, preferred_element_type=jnp.float32)
    query_heads = queries.reshape(block_count, block_rows, local_heads, HEAD_DIM)
    score_scale = HEAD_DIM ** (-0.5)
    scores = (
        jnp.einsum("bqhd,bkhd->bhqk", query_heads, key_heads, preferred_element_type=jnp.float32)
        * score_scale
    )
    probs = jax.nn.softmax(scores, axis=-1)
    probs_low = probs.astype(jnp.bfloat16)
    attended = jnp.einsum(
        "bhqk,bkhd->bqhd", probs_low, value_heads, preferred_element_type=jnp.float32
    ).reshape(tokens_here, local_width)
    gate_sigmoid = jax.nn.sigmoid(gates)
    upstream = output_grad.astype(jnp.float32)
    d_attended = (upstream * gates * gate_sigmoid).astype(jnp.bfloat16)
    d_gates = (upstream * attended * gate_sigmoid * (1.0 + gates * (1.0 - gate_sigmoid))).astype(
        jnp.bfloat16
    )
    d_heads = d_attended.reshape(block_count, block_rows, local_heads, HEAD_DIM)
    d_probs = jnp.einsum(
        "bqhd,bkhd->bhqk", d_heads, value_heads, preferred_element_type=jnp.float32
    )
    centre = jnp.sum(probs * d_probs, axis=-1, keepdims=True)
    d_scores = (probs * (d_probs - centre) * score_scale).astype(jnp.bfloat16)
    d_queries = (
        jnp.einsum("bhqk,bkhd->bqhd", d_scores, key_heads, preferred_element_type=jnp.float32)
        .astype(jnp.bfloat16)
        .reshape(tokens_here, local_width)
    )
    d_block_keys = jnp.einsum(
        "bhqk,bqhd->bkhd", d_scores, query_heads, preferred_element_type=jnp.float32
    ).reshape(requests, span_rows, local_width)
    d_block_values = jnp.einsum(
        "bhqk,bqhd->bkhd", probs_low, d_heads, preferred_element_type=jnp.float32
    ).reshape(requests, span_rows, local_width)
    contract = (((1,), (1,)), ((), ()))
    slot_total = owner_count * capacity
    back_keys = (
        jnp.zeros((slot_total, span_rows, local_width), jnp.float32).at[slot_flat].set(d_block_keys)
    )
    back_values = (
        jnp.zeros((slot_total, span_rows, local_width), jnp.float32)
        .at[slot_flat]
        .set(d_block_values)
    )
    came_dkeys, came_dvalues = (
        lax.all_to_all(
            back_keys.reshape(owner_count, capacity, span_rows, local_width),
            "st",
            split_axis=0,
            concat_axis=0,
            tiled=True,
        ),
        lax.all_to_all(
            back_values.reshape(owner_count, capacity, span_rows, local_width),
            "st",
            split_axis=0,
            concat_axis=0,
            tiled=True,
        ),
    )
    slot_owner = jnp.where(filled, slot_table, -1).reshape(slot_total)
    selector = (jnp.arange(held_count, dtype=jnp.int32)[:, None] == slot_owner[None, :]).astype(
        jnp.float32
    )
    key_totals = jnp.dot(
        selector,
        came_dkeys.reshape(slot_total, span_rows * local_width),
        precision=lax.Precision.HIGHEST,
        preferred_element_type=jnp.float32,
    )
    value_totals = jnp.dot(
        selector,
        came_dvalues.reshape(slot_total, span_rows * local_width),
        precision=lax.Precision.HIGHEST,
        preferred_element_type=jnp.float32,
    )
    key_low = key_totals.astype(jnp.bfloat16).reshape(held_count, span_rows, local_width)
    value_low = value_totals.astype(jnp.bfloat16).reshape(held_count, span_rows, local_width)
    weight_part = lax.dot_general(
        store_rows,
        value_low.reshape(held_count * span_rows, local_width),
        (((0,), (0,)), ((), ())),
        preferred_element_type=jnp.float32,
    )
    grad_value_weight = lax.psum(weight_part, "st")
    grad_hidden = lax.psum_scatter(
        lax.dot_general(d_queries, query_weight, contract, preferred_element_type=jnp.float32)
        + lax.dot_general(d_gates, gate_weight, contract, preferred_element_type=jnp.float32),
        "tp",
        scatter_dimension=0,
        tiled=True,
    ).astype(jnp.bfloat16)
    rows_key = key_low.reshape(
        held_count // lax.axis_size("tp") * lax.axis_size("tp") * span_rows, local_width
    )
    rows_value = value_low.reshape(
        held_count // lax.axis_size("tp") * lax.axis_size("tp") * span_rows, local_width
    )
    summed = lax.dot_general(
        rows_key, key_weight, contract, preferred_element_type=jnp.float32
    ) + lax.dot_general(rows_value, value_weight, contract, preferred_element_type=jnp.float32)
    grad_store = lax.psum_scatter(
        summed.reshape(
            held_count // lax.axis_size("tp") * lax.axis_size("tp"), span_rows, model_width
        ),
        "tp",
        scatter_dimension=0,
        tiled=True,
    ).astype(jnp.bfloat16)
    return (grad_hidden, grad_store, grad_value_weight)


def solution(mesh):
    placed = (
        P("st", None),
        P("st", None, None),
        P("st", None),
        P(None, "tp"),
        P(None, "tp"),
        P(None, "tp"),
        P(None, "tp"),
        P("st", "tp"),
    )
    return jax.shard_map(
        body,
        mesh=mesh,
        in_specs=placed,
        out_specs=(P(("st", "tp"), None), P(("st", "tp"), None, None), P(None, "tp")),
        check_vma=False,
    )
```

profile of v0, /device:TPU:0, one launch (start us, length us, event | category | flops | bytes accessed | tf_op | source)
XLA Modules:
  0.0 531.6 jit_solution(4978605036159977339)
XLA Ops:
  8.0 0.0 copy-start
  8.0 42.9 %all-gather = s32[16,8,4]{1,2,0:T(4,128)S(1)} all-gather(s32[1,8,4]{1,2,0:T(4,128)} %bitcast.110), channel_id=1, replica_groups=mesh['st'=16,'tp'=2] {'st'}, dimensions={0}, use_global_device_ids=true | all-gather | bytes 2176 | tf_op jit(solution)/shard_map/all_gather | solution.py:32
  51.0 0.1 copy.41
  51.1 0.1 copy.42
  51.2 0.5 convert_reduce_fusion
  51.6 0.2 select_reduce_fusion
  51.8 0.1 copy.46
  51.9 0.1 reshape.296
  52.0 6.0 %convolution_convert_fusion.2 = bf16[2048,256]{1,0:T(8,128)(2,1)S(1)} fusion(bf16[2048,2048]{1,0:T(8,128)(2,1)} %bitcast.89, bf16[2048,256]{1,0:T(8,128)(2,1)} %param.14), kind=kOutput, calls=%fused_computation.13 | convolution fusion | flops 2148007936 | bytes 10485760 | tf_op jit(solution)/shard_map/dot_general | solution.py:55
  58.0 2.0 gather_fusion.2
  60.0 4.4 all-to-all-start.1
  64.4 6.0 %convolution_convert_fusion.3 = bf16[2048,256]{1,0:T(8,128)(2,1)S(1)} fusion(bf16[2048,2048]{1,0:T(8,128)(2,1)} %bitcast.90, bf16[2048,256]{1,0:T(8,128)(2,1)} %param.13), kind=kOutput, calls=%fused_computation.14 | convolution fusion | flops 2148007936 | bytes 10485760 | tf_op jit(solution)/shard_map/dot_general | solution.py:50
  70.4 2.0 gather_fusion
  72.4 30.7 %all-to-all-done.1 = bf16[16,4,64,256]{3,2,1,0:T(8,128)(2,1)} async-done(((bf16[16,4,64,256]{3,2,1,0:T(8,128)(2,1)}), bf16[16,4,64,256]{3,2,1,0:T(8,128)(2,1)}, u32[]{:S(2)}, u32[]{:S(2)}) %all-to-all-start.1) | async-done | bytes 2097184 | tf_op jit(solution)/shard_map/all_to_all | solution.py:61
  103.1 7.6 %all-to-all-start = ((bf16[16,4,64,256]{3,2,1,0:T(8,128)(2,1)}), bf16[16,4,64,256]{3,2,1,0:T(8,128)(2,1)}, u32[]{:S(2)}, u32[]{:S(2)}) async-start(bf16[16,4,64,256]{3,2,1,0:T(8,128)(2,1)} %bitcast.95), calls=%async_computation | async-start | bytes 4194304 | tf_op jit(solution)/shard_map/all_to_all | solution.py:60
  110.7 0.7 convolution_convert_fusion.5
  111.4 3.3 gather_fusion.3
  114.7 36.4 %all-to-all-done = bf16[16,4,64,256]{3,2,1,0:T(8,128)(2,1)} async-done(((bf16[16,4,64,256]{3,2,1,0:T(8,128)(2,1)}), bf16[16,4,64,256]{3,2,1,0:T(8,128)(2,1)}, u32[]{:S(2)}, u32[]{:S(2)}) %all-to-all-start) | async-done | bytes 2097184 | tf_op jit(solution)/shard_map/all_to_all | solution.py:60
  151.1 2.2 gather_fusion.1
  153.3 0.4 convolution_multiply_fusion
  153.8 0.8 copy-done.3
  154.5 0.9 fusion.35
  155.5 3.3 fusion.22
  158.8 3.1 fusion.17
  161.9 1.2 fusion.36
  163.1 4.9 fusion.8
  168.0 2.5 broadcast.191.clone
  170.6 5.3 %scatter_fusion = f32[64,64,256]{2,1,0:T(8,128)} fusion(f32[64,64,256]{2,1,0:T(8,128)} %broadcast.191.clone, s32[32]{0:T(128)S(1)} %fusion.30, f32[32,64,256]{2,1,0:T(8,128)S(1)} %bitcast.103), kind=kCustom, calls=%fused_computation.4 | custom fusion | bytes 6291584 | tf_op jit(solution)/shard_map/scatter | solution.py:106
  175.9 9.8 %all-to-all-start.2 = ((f32[16,4,64,256]{3,2,1,0:T(8,128)}), f32[16,4,64,256]{3,2,1,0:T(8,128)}, u32[]{:S(2)}, u32[]{:S(2)}) async-start(f32[16,4,64,256]{3,2,1,0:T(8,128)} %bitcast.88), calls=%async_computation.3 | async-start | bytes 8388608 | tf_op jit(solution)/shard_map/all_to_all | solution.py:114
  185.8 2.6 fusion.20
  188.3 2.5 broadcast.191.clone.1
  190.8 5.4 %scatter_fusion.1 = f32[64,64,256]{2,1,0:T(8,128)} fusion(f32[64,64,256]{2,1,0:T(8,128)} %broadcast.191.clone.1, s32[32]{0:T(128)S(1)} %fusion.30, f32[32,64,256]{2,1,0:T(8,128)S(1)} %bitcast.94), kind=kCustom, calls=%fused_computation.5 | custom fusion | bytes 6291584 | tf_op jit(solution)/shard_map/scatter | solution.py:111
  196.2 4.2 convolution_convert_fusion.4
  200.4 63.6 %all-to-all-done.2 = f32[16,4,64,256]{3,2,1,0:T(8,128)} async-done(((f32[16,4,64,256]{3,2,1,0:T(8,128)}), f32[16,4,64,256]{3,2,1,0:T(8,128)}, u32[]{:S(2)}, u32[]{:S(2)}) %all-to-all-start.2) | async-done | bytes 4194336 | tf_op jit(solution)/shard_map/all_to_all | solution.py:114
  264.0 19.2 %all-to-all-start.3 = ((f32[16,4,64,256]{3,2,1,0:T(8,128)}), f32[16,4,64,256]{3,2,1,0:T(8,128)}, u32[]{:S(2)}, u32[]{:S(2)}) async-start(f32[16,4,64,256]{3,2,1,0:T(8,128)} %bitcast.87), calls=%async_computation.4 | async-start | bytes 8388608 | tf_op jit(solution)/shard_map/all_to_all | solution.py:121
  283.2 0.0 copy-start.4
  283.2 0.0 reduce-scatter.3.cloned.1.call-start
  283.3 0.7 fusion.37
  284.0 0.4 copy-done.4
  284.4 0.0 copy-done.7
  284.5 2.8 convolution_add_fusion.1
  287.3 0.0 reduce-scatter.3.cloned.1.call-update
  287.4 0.0 all-reduce.2.cloned.1.call-start
  287.4 0.1 fusion.25
  287.6 0.1 copy.47
  287.6 0.1 select_n.78
  287.7 6.5 %copy.49 = f32[8,8,64,256]{3,1,2,0:T(8,128)} copy(f32[8,8,64,256]{3,2,1,0:T(8,128)} %bitcast.42) | data formatting | bytes 8388608
  294.3 67.3 %all-to-all-done.3 = f32[16,4,64,256]{3,2,1,0:T(8,128)} async-done(((f32[16,4,64,256]{3,2,1,0:T(8,128)}), f32[16,4,64,256]{3,2,1,0:T(8,128)}, u32[]{:S(2)}, u32[]{:S(2)}) %all-to-all-start.3) | async-done | bytes 4194336 | tf_op jit(solution)/shard_map/all_to_all | solution.py:121
  361.6 4.6 copy.50
  366.1 1.6 convolution_convert_fusion
  367.8 0.5 reshape_reshape.8
  368.3 7.0 %convolution_bitcast_fusion = f32[2048,256]{0,1:T(8,128)} fusion(bf16[2048,256]{1,0:T(8,128)(2,1)S(1)} %reshape_reshape.8, bf16[2048,2048]{1,0:T(8,128)(2,1)} %bitcast.91), kind=kOutput, calls=%fused_computation.12 | convolution fusion | flops 2147483648 | bytes 11534336 | tf_op jit(solution)/shard_map/dot_general | solution.py:147
  375.4 0.0 all-reduce.2.cloned.1.call-update
  375.4 0.3 reduce-scatter.5.cloned.1.call-start
  375.6 3.8 convolution_convert_fusion.1
  379.4 0.5 reshape_reshape.7
  380.0 3.6 fusion.38
  383.6 9.7 %convolution_add_fusion = f32[2048,2048]{1,0:T(8,128)} fusion(f32[2048,2048]{1,0:T(8,128)S(1)} %fusion.38, bf16[2048,256]{1,0:T(8,128)(2,1)S(1)} %reshape_reshape.8, bf16[2048,256]{1,0:T(8,128)(2,1)} %param.14), kind=kOutput, calls=%fused_computation.10 | convolution fusion | flops 2151677952 | bytes 35651584 | tf_op jit(solution)/shard_map/dot_general | solution.py:169
  393.3 0.0 reduce-scatter.5.cloned.1.call-update
  393.3 0.0 reduce-scatter.3.cloned.1.call-done
  393.4 3.0 convert_element_type.63
  396.4 118.7 %all-reduce.2.cloned.1.call-done = f32[2048,256]{0,1:T(8,128)} async-done(((f32[2048,256]{0,1:T(8,128)}), f32[2048,256]{0,1:T(8,128)}) %all-reduce.2.cloned.1.call-update) | async-done | bytes 2097168 | tf_op jit(solution)/shard_map/psum | solution.py:153
  515.1 3.0 copy.48
  518.1 6.0 %convert_element_type.66 = bf16[16,64,2048]{2,1,0:T(8,128)(2,1)} convert(f32[16,64,2048]{2,1,0:T(8,128)} %reduce-scatter.5.cloned.1.call-done) | non-fusion elementwise | flops 2097152 | bytes 12582912 | tf_op jit(solution)/shard_map/convert_element_type | solution.py:177
  (22 shorter events, 0.1 us)
Async XLA Ops:
  8.0 102.7 %copy-start = (bf16[512,2048]{1,0:T(8,128)(2,1)S(1)}, bf16[512,2048]{1,0:T(8,128)(2,1)}, u32[]{:S(2)}) copy-start(bf16[512,2048]{1,0:T(8,128)(2,1)} %param.8) | copy-start | bytes 6291460
  60.0 43.1 %all-to-all-start.1 = ((bf16[16,4,64,256]{3,2,1,0:T(8,128)(2,1)}), bf16[16,4,64,256]{3,2,1,0:T(8,128)(2,1)}, u32[]{:S(2)}, u32[]{:S(2)}) async-start(bf16[16,4,64,256]{3,2,1,0:T(8,128)(2,1)} %bitcast.96), calls=%async_computation.1 | async-start | bytes 4194304 | tf_op jit(solution)/shard_map/all_to_all | solution.py:61
  72.4 38.3 %copy-start.5 = (bf16[2048,256]{1,0:T(8,128)(2,1)S(1)}, bf16[2048,256]{1,0:T(8,128)(2,1)}, u32[]{:S(2)}) copy-start(bf16[2048,256]{1,0:T(8,128)(2,1)} %param.11) | copy-start | bytes 3145732
  103.1 48.0 %all-to-all-start = ((bf16[16,4,64,256]{3,2,1,0:T(8,128)(2,1)}), bf16[16,4,64,256]{3,2,1,0:T(8,128)(2,1)}, u32[]{:S(2)}, u32[]{:S(2)}) async-start(bf16[16,4,64,256]{3,2,1,0:T(8,128)(2,1)} %bitcast.95), calls=%async_computation | async-start | bytes 4194304 | tf_op jit(solution)/shard_map/all_to_all | solution.py:60
  111.4 44.1 %copy-start.8 = (bf16[512,256]{1,0:T(8,128)(2,1)}, bf16[512,256]{1,0:T(8,128)(2,1)S(1)}, u32[]{:S(2)}) copy-start(bf16[512,256]{1,0:T(8,128)(2,1)S(1)} %convolution_convert_fusion.5) | copy-start | bytes 786436
  153.7 0.8 copy-start.3
  158.8 3.1 copy-start.2
  175.9 88.1 %all-to-all-start.2 = ((f32[16,4,64,256]{3,2,1,0:T(8,128)}), f32[16,4,64,256]{3,2,1,0:T(8,128)}, u32[]{:S(2)}, u32[]{:S(2)}) async-start(f32[16,4,64,256]{3,2,1,0:T(8,128)} %bitcast.88), calls=%async_computation.3 | async-start | bytes 8388608 | tf_op jit(solution)/shard_map/all_to_all | solution.py:114
  264.0 19.3 %copy-start.6 = (bf16[2048,256]{1,0:T(8,128)(2,1)S(1)}, bf16[2048,256]{1,0:T(8,128)(2,1)}, u32[]{:S(2)}) copy-start(bf16[2048,256]{1,0:T(8,128)(2,1)} %param.11) | copy-start | bytes 3145732
  264.0 97.6 %all-to-all-start.3 = ((f32[16,4,64,256]{3,2,1,0:T(8,128)}), f32[16,4,64,256]{3,2,1,0:T(8,128)}, u32[]{:S(2)}, u32[]{:S(2)}) async-start(f32[16,4,64,256]{3,2,1,0:T(8,128)} %bitcast.87), calls=%async_computation.4 | async-start | bytes 8388608 | tf_op jit(solution)/shard_map/all_to_all | solution.py:121
  283.2 1.2 copy-start.4
  283.2 1.3 copy-start.7
  283.2 110.1 %reduce-scatter.3.cloned.1.call-start = ((), (), s32[]{:S(2)}) async-start(), calls=%async_computation.6 | async-start | bytes 6291456 | tf_op jit(solution)/shard_map/reduce_scatter | solution.py:154
  287.4 227.7 %all-reduce.2.cloned.1.call-start = ((), (), s32[]{:S(2)}) async-start(), calls=%async_computation.8 | async-start | bytes 4194304 | tf_op jit(solution)/shard_map/psum | solution.py:153
  375.4 142.7 %reduce-scatter.5.cloned.1.call-start = ((), (), s32[]{:S(2)}) async-start(), calls=%async_computation.7 | async-start | bytes 25165824 | tf_op jit(solution)/shard_map/reduce_scatter | solution.py:170
  515.1 9.1 %copy-start.1 = (bf16[512,2048]{1,0:T(8,128)(2,1)S(1)}, bf16[512,2048]{1,0:T(8,128)(2,1)}, u32[]{:S(2)}) copy-start(bf16[512,2048]{1,0:T(8,128)(2,1)} %param.8) | copy-start | bytes 6291460
Sparse Core Ops, SparseCore 0:
  287.5 13.2 reduce-scatter.2
  393.5 38.9 reduce-scatter.4
Sparse Core Ops, SparseCore 1:
  375.5 139.5 all-reduce.1
where the time goes:
time: 533 us; the launch traced here: 532 us
  waiting for transfers between devices  317 us (59%)
  matrix products  61.7 us (12%)
  blocking collectives  42.9 us (8%)
  local copies, waits for them, and re-layouts  42.2 us (8%)
  starting transfers between devices  41.4 us (8%)
  between operations  15.7 us (3%)
  other arithmetic  10.9 us (2%)
    psum x1, waiting for transfers between devices, body(): grad_value_weight = lax.psum(weight_part, 'st')  119 us
    all_to_all x1, waiting for transfers between devices, body(): lax.all_to_all(back_values.reshape(owner_count, capacity, span_rows, loca...  67.3 us
    all_to_all x1, waiting for transfers between devices, body(): lax.all_to_all(back_keys.reshape(owner_count, capacity, span_rows, local_...  63.6 us
    all_gather x1, blocking collectives, body(): lax.all_gather(passage_ids, 'st', axis=0, tiled=True)  42.9 us
    all_to_all x1, waiting for transfers between devices, body(): lax.all_to_all(keys_here[slot_table], 'st', split_axis=0, concat_axis=0,...  36.4 us
    all_to_all x1, waiting for transfers between devices, body(): lax.all_to_all(values_here[slot_table], 'st', split_axis=0, concat_axis=0...  30.7 us
    all_to_all x1, starting transfers between devices, body(): lax.all_to_all(back_values.reshape(owner_count, capacity, span_rows, loca...  19.2 us
    unnamed x21, local copies, waits for them, and re-layouts  15.4 us
  transfers between devices with their start and end apart: 7, of which 5 were waited for; matrix products, arithmetic and copies ran while one was open for 14% of the time, Pallas kernels for 0%

commit v1 on v0

--- a/solution.py
+++ b/solution.py
@@ -4,6 +4,14 @@
 from jax.sharding import PartitionSpec as P
 
 HEAD_DIM = 256
+
+
+def add_in_pairs(array, mesh_axis):
+    size, acc = (lax.axis_size(mesh_axis), array)
+    for hop in [1 << k for k in range(size.bit_length() - 1)]:
+        pairs = [(i, i ^ hop) for i in range(size)]
+        acc = acc + lax.ppermute(acc, mesh_axis, pairs)
+    return acc
 
 
 def body(
@@ -150,7 +158,7 @@
         (((0,), (0,)), ((), ())),
         preferred_element_type=jnp.float32,
     )
-    grad_value_weight = lax.psum(weight_part, "st")
+    grad_value_weight = add_in_pairs(weight_part, "st")
     grad_hidden = lax.psum_scatter(
         lax.dot_general(d_queries, query_weight, contract, preferred_element_type=jnp.float32)
         + lax.dot_general(d_gates, gate_weight, contract, preferred_element_type=jnp.float32),

time: 533 us -> 651 us (1.22)
  waiting for transfers between devices: 317 us -> 417 us
  starting transfers between devices: 41.4 us -> 62.5 us
    ppermute x0 -> x4, waiting for transfers between devices: none -> 219 us  [add_in_pairs(): acc = acc + lax.ppermute(acc, mesh_axis, pairs)]
    psum x1 -> x0, waiting for transfers between devices: 119 us -> none  [body(): grad_value_weight = lax.psum(weight_part, 'st')]
    ppermute x0 -> x4, starting transfers between devices: none -> 21.3 us  [add_in_pairs(): acc = acc + lax.ppermute(acc, mesh_axis, pairs)]
  transfers between devices with their start and end apart: 7 -> 10, of which waited for: 5 -> 8; matrix products, arithmetic and copies ran while one was open for 14% -> 11% of each run, Pallas kernels for 0% -> 0%
where the time goes in v1:
time: 651 us; the launch traced here: 650 us
  waiting for transfers between devices  417 us (64%)
  starting transfers between devices  62.5 us (10%)
  matrix products  58.2 us (9%)
  blocking collectives  42.9 us (7%)
  local copies, waits for them, and re-layouts  40.3 us (6%)
  other arithmetic  14.7 us (2%)
  between operations  14.3 us (2%)
    ppermute x4, waiting for transfers between devices, add_in_pairs(): acc = acc + lax.ppermute(acc, mesh_axis, pairs)  219 us
    all_to_all x1, waiting for transfers between devices, body(): lax.all_to_all(back_keys.reshape(owner_count, capacity, span_rows, local_...  67.8 us
    all_to_all x1, waiting for transfers between devices, body(): lax.all_to_all(back_values.reshape(owner_count, capacity, span_rows, loca...  62.9 us
    all_gather x1, blocking collectives, body(): lax.all_gather(passage_ids, 'st', axis=0, tiled=True)  42.9 us
    all_to_all x1, waiting for transfers between devices, body(): lax.all_to_all(keys_here[slot_table], 'st', split_axis=0, concat_axis=0,...  36.4 us
    all_to_all x1, waiting for transfers between devices, body(): lax.all_to_all(values_here[slot_table], 'st', split_axis=0, concat_axis=0...  30.7 us
    ppermute x4, starting transfers between devices, add_in_pairs(): acc = acc + lax.ppermute(acc, mesh_axis, pairs)  21.3 us
    all_to_all x1, starting transfers between devices, body(): lax.all_to_all(back_values.reshape(owner_count, capacity, span_rows, loca...  19.1 us
  transfers between devices with their start and end apart: 10, of which 8 were waited for; matrix products, arithmetic and copies ran while one was open for 11% of the time, Pallas kernels for 0%

profile of v1, /device:TPU:0, one launch (start us, length us, event | category | flops | bytes accessed | tf_op | source)
XLA Modules:
  0.0 649.9 jit_solution(15690118481992731476)
XLA Ops:
  7.2 42.9 %all-gather = s32[16,8,4]{1,2,0:T(4,128)S(1)} all-gather(s32[1,8,4]{1,2,0:T(4,128)} %bitcast.110), channel_id=1, replica_groups=mesh['st'=16,'tp'=2] {'st'}, dimensions={0}, use_global_device_ids=true | all-gather | bytes 2176 | tf_op jit(solution)/shard_map/all_gather | solution.py:40
  50.1 0.1 copy.41
  50.3 0.5 convert_reduce_fusion
  50.8 0.2 select_reduce_fusion
  51.0 0.1 copy.46
  51.0 0.1 reshape.296
  51.2 6.0 convolution_convert_fusion.2
  57.1 2.0 gather_fusion.2
  59.1 4.4 all-to-all-start.1
  63.6 6.0 convolution_convert_fusion.3
  69.5 2.0 gather_fusion
  71.5 30.7 %all-to-all-done.1 = bf16[16,4,64,256]{3,2,1,0:T(8,128)(2,1)} async-done(((bf16[16,4,64,256]{3,2,1,0:T(8,128)(2,1)}), bf16[16,4,64,256]{3,2,1,0:T(8,128)(2,1)}, u32[]{:S(2)}, u32[]{:S(2)}) %all-to-all-start.1) | async-done | bytes 2097184 | tf_op jit(solution)/shard_map/all_to_all | solution.py:69
  102.2 7.7 %all-to-all-start = ((bf16[16,4,64,256]{3,2,1,0:T(8,128)(2,1)}), bf16[16,4,64,256]{3,2,1,0:T(8,128)(2,1)}, u32[]{:S(2)}, u32[]{:S(2)}) async-start(bf16[16,4,64,256]{3,2,1,0:T(8,128)(2,1)} %bitcast.95), calls=%async_computation | async-start | bytes 4194304 | tf_op jit(solution)/shard_map/all_to_all | solution.py:68
  110.0 0.7 convolution_convert_fusion.5
  110.7 3.3 gather_fusion.3
  114.0 36.4 %all-to-all-done = bf16[16,4,64,256]{3,2,1,0:T(8,128)(2,1)} async-done(((bf16[16,4,64,256]{3,2,1,0:T(8,128)(2,1)}), bf16[16,4,64,256]{3,2,1,0:T(8,128)(2,1)}, u32[]{:S(2)}, u32[]{:S(2)}) %all-to-all-start) | async-done | bytes 2097184 | tf_op jit(solution)/shard_map/all_to_all | solution.py:68
  150.4 2.2 gather_fusion.1
  152.6 0.4 convolution_multiply_fusion
  153.1 0.8 copy-done.3
  153.8 0.9 fusion.35
  154.8 3.3 fusion.22
  158.1 3.1 fusion.17
  161.2 1.2 fusion.36
  162.4 4.9 fusion.8
  167.3 2.5 broadcast.191.clone
  169.9 5.3 scatter_fusion
  175.2 9.9 %all-to-all-start.2 = ((f32[16,4,64,256]{3,2,1,0:T(8,128)}), f32[16,4,64,256]{3,2,1,0:T(8,128)}, u32[]{:S(2)}, u32[]{:S(2)}) async-start(f32[16,4,64,256]{3,2,1,0:T(8,128)} %bitcast.88), calls=%async_computation.3 | async-start | bytes 8388608 | tf_op jit(solution)/shard_map/all_to_all | solution.py:122
  185.1 2.5 fusion.20
  187.6 2.5 broadcast.191.clone.1
  190.1 5.4 scatter_fusion.1
  195.5 67.8 %all-to-all-done.2 = f32[16,4,64,256]{3,2,1,0:T(8,128)} async-done(((f32[16,4,64,256]{3,2,1,0:T(8,128)}), f32[16,4,64,256]{3,2,1,0:T(8,128)}, u32[]{:S(2)}, u32[]{:S(2)}) %all-to-all-start.2) | async-done | bytes 4194336 | tf_op jit(solution)/shard_map/all_to_all | solution.py:122
  263.3 19.1 %all-to-all-start.3 = ((f32[16,4,64,256]{3,2,1,0:T(8,128)}), f32[16,4,64,256]{3,2,1,0:T(8,128)}, u32[]{:S(2)}, u32[]{:S(2)}) async-start(f32[16,4,64,256]{3,2,1,0:T(8,128)} %bitcast.87), calls=%async_computation.4 | async-start | bytes 8388608 | tf_op jit(solution)/shard_map/all_to_all | solution.py:129
  282.4 4.2 convolution_convert_fusion.4
  286.7 0.7 fusion.37
  287.4 0.5 copy-done.4
  287.9 2.8 convolution_add_fusion.1
  290.8 0.1 fusion.25
  290.9 0.1 copy.47
  291.0 0.1 select_n.78
  291.1 4.6 copy.49
  295.7 1.6 convolution_convert_fusion.1
  297.3 0.5 reshape_reshape.7
  297.9 62.9 %all-to-all-done.3 = f32[16,4,64,256]{3,2,1,0:T(8,128)} async-done(((f32[16,4,64,256]{3,2,1,0:T(8,128)}), f32[16,4,64,256]{3,2,1,0:T(8,128)}, u32[]{:S(2)}, u32[]{:S(2)}) %all-to-all-start.3) | async-done | bytes 4194336 | tf_op jit(solution)/shard_map/all_to_all | solution.py:129
  360.7 4.6 copy.50
  365.3 1.6 convolution_convert_fusion
  366.9 0.7 reshape_reshape.8
  367.7 3.6 fusion.38
  371.3 9.7 %convolution_add_fusion = f32[2048,2048]{1,0:T(8,128)} fusion(f32[2048,2048]{1,0:T(8,128)S(1)} %fusion.38, bf16[2048,256]{1,0:T(8,128)(2,1)S(1)} %reshape_reshape.8, bf16[2048,256]{1,0:T(8,128)(2,1)} %param.14), kind=kOutput, calls=%fused_computation.10 | convolution fusion | flops 2151677952 | bytes 35651584 | tf_op jit(solution)/shard_map/dot_general | solution.py:177
  381.0 5.7 convolution_bitcast_fusion
  386.8 2.2 collective-permute-start
  388.9 43.9 %collective-permute-done = f32[2048,256]{0,1:T(8,128)S(1)} collective-permute-done((f32[2048,256]{0,1:T(8,128)S(1)}, f32[2048,256]{0,1:T(8,128)S(1)}, u32[]{:S(2)}, u32[]{:S(2)}) %collective-permute-start) | collective-permute-done | bytes 2097184 | tf_op jit(solution)/shard_map/ppermute | solution.py:13
  432.8 0.2 add.102
  433.0 6.2 collective-permute-start.1
  439.3 43.3 %collective-permute-done.1 = f32[2048,256]{0,1:T(8,128)S(1)} collective-permute-done((f32[2048,256]{0,1:T(8,128)S(1)}, f32[2048,256]{0,1:T(8,128)S(1)}, u32[]{:S(2)}, u32[]{:S(2)}) %collective-permute-start.1) | collective-permute-done | bytes 2097184 | tf_op jit(solution)/shard_map/ppermute | solution.py:13
  482.6 0.3 add.103
  482.9 12.9 %collective-permute-start.2 = (f32[2048,256]{0,1:T(8,128)S(1)}, f32[2048,256]{0,1:T(8,128)S(1)}, u32[]{:S(2)}, u32[]{:S(2)}) collective-permute-start(f32[2048,256]{0,1:T(8,128)S(1)} %add.103), channel_id=1, source_target_pairs={{0,8},{2,10},{4,12},{6,14},{8,0},{10,2},{12,4},{14,6},{16,24},{18,... | collective-permute-start | bytes 6291464 | tf_op jit(solution)/shard_map/ppermute | solution.py:13
  495.8 44.2 %collective-permute-done.2 = f32[2048,256]{0,1:T(8,128)S(1)} collective-permute-done((f32[2048,256]{0,1:T(8,128)S(1)}, f32[2048,256]{0,1:T(8,128)S(1)}, u32[]{:S(2)}, u32[]{:S(2)}) %collective-permute-start.2) | collective-permute-done | bytes 2097184 | tf_op jit(solution)/shard_map/ppermute | solution.py:13
  540.0 0.2 add.104
  540.2 0.1 collective-permute-start.3
  540.3 2.7 convert_element_type.63
  543.0 87.7 %collective-permute-done.3 = f32[2048,256]{0,1:T(8,128)} collective-permute-done((f32[2048,256]{0,1:T(8,128)S(1)}, f32[2048,256]{0,1:T(8,128)}, u32[]{:S(2)}, u32[]{:S(2)}) %collective-permute-start.3) | collective-permute-done | bytes 2097184 | tf_op jit(solution)/shard_map/ppermute | solution.py:13
  630.7 3.2 add.105
  634.0 2.9 copy.48
  636.9 6.2 convert_element_type.66
  (31 shorter events, 0.4 us)
Async XLA Ops:
  7.2 102.8 %copy-start = (bf16[512,2048]{1,0:T(8,128)(2,1)S(1)}, bf16[512,2048]{1,0:T(8,128)(2,1)}, u32[]{:S(2)}) copy-start(bf16[512,2048]{1,0:T(8,128)(2,1)} %param.8) | copy-start | bytes 6291460
  59.1 43.1 %all-to-all-start.1 = ((bf16[16,4,64,256]{3,2,1,0:T(8,128)(2,1)}), bf16[16,4,64,256]{3,2,1,0:T(8,128)(2,1)}, u32[]{:S(2)}, u32[]{:S(2)}) async-start(bf16[16,4,64,256]{3,2,1,0:T(8,128)(2,1)} %bitcast.96), calls=%async_computation.1 | async-start | bytes 4194304 | tf_op jit(solution)/shard_map/all_to_all | solution.py:69
  102.2 7.8 %copy-start.5 = (bf16[2048,256]{1,0:T(8,128)(2,1)S(1)}, bf16[2048,256]{1,0:T(8,128)(2,1)}, u32[]{:S(2)}) copy-start(bf16[2048,256]{1,0:T(8,128)(2,1)} %param.11) | copy-start | bytes 3145732
  102.2 48.2 %all-to-all-start = ((bf16[16,4,64,256]{3,2,1,0:T(8,128)(2,1)}), bf16[16,4,64,256]{3,2,1,0:T(8,128)(2,1)}, u32[]{:S(2)}, u32[]{:S(2)}) async-start(bf16[16,4,64,256]{3,2,1,0:T(8,128)(2,1)} %bitcast.95), calls=%async_computation | async-start | bytes 4194304 | tf_op jit(solution)/shard_map/all_to_all | solution.py:68
  110.7 41.9 %copy-start.8 = (bf16[512,256]{1,0:T(8,128)(2,1)}, bf16[512,256]{1,0:T(8,128)(2,1)S(1)}, u32[]{:S(2)}) copy-start(bf16[512,256]{1,0:T(8,128)(2,1)S(1)} %convolution_convert_fusion.5) | copy-start | bytes 786436
  153.1 0.8 copy-start.3
  158.1 3.1 copy-start.2
  175.2 88.1 %all-to-all-start.2 = ((f32[16,4,64,256]{3,2,1,0:T(8,128)}), f32[16,4,64,256]{3,2,1,0:T(8,128)}, u32[]{:S(2)}, u32[]{:S(2)}) async-start(f32[16,4,64,256]{3,2,1,0:T(8,128)} %bitcast.88), calls=%async_computation.3 | async-start | bytes 8388608 | tf_op jit(solution)/shard_map/all_to_all | solution.py:122
  263.3 97.4 %all-to-all-start.3 = ((f32[16,4,64,256]{3,2,1,0:T(8,128)}), f32[16,4,64,256]{3,2,1,0:T(8,128)}, u32[]{:S(2)}, u32[]{:S(2)}) async-start(f32[16,4,64,256]{3,2,1,0:T(8,128)} %bitcast.87), calls=%async_computation.4 | async-start | bytes 8388608 | tf_op jit(solution)/shard_map/all_to_all | solution.py:129
  282.4 4.3 copy-start.6
  282.4 257.9 %reduce-scatter.3.cloned.1.call-start = ((), (), s32[]{:S(2)}) async-start(), calls=%async_computation.6 | async-start | bytes 6291456 | tf_op jit(solution)/shard_map/reduce_scatter | solution.py:162
  286.7 1.2 copy-start.4
  286.7 1.3 copy-start.7
  290.7 346.1 %reduce-scatter.5.cloned.1.call-start = ((), (), s32[]{:S(2)}) async-start(), calls=%async_computation.7 | async-start | bytes 25165824 | tf_op jit(solution)/shard_map/reduce_scatter | solution.py:178
  386.8 46.0 %collective-permute-start = (f32[2048,256]{0,1:T(8,128)S(1)}, f32[2048,256]{0,1:T(8,128)S(1)}, u32[]{:S(2)}, u32[]{:S(2)}) collective-permute-start(f32[2048,256]{0,1:T(8,128)S(1)} %convolution_bitcast_fusion), channel_id=1, source_target_pairs={{0,2},{2,0},{4,6},{6,4},{8,10},{10,8},{12,14},{14,12},{16,18},{18,... | collective-permute-start | bytes 6291464 | tf_op jit(solution)/shard_map/ppermute | solution.py:13
  433.0 49.6 %collective-permute-start.1 = (f32[2048,256]{0,1:T(8,128)S(1)}, f32[2048,256]{0,1:T(8,128)S(1)}, u32[]{:S(2)}, u32[]{:S(2)}) collective-permute-start(f32[2048,256]{0,1:T(8,128)S(1)} %add.102), channel_id=1, source_target_pairs={{0,4},{2,6},{4,0},{6,2},{8,12},{10,14},{12,8},{14,10},{16,20},{18,... | collective-permute-start | bytes 6291464 | tf_op jit(solution)/shard_map/ppermute | solution.py:13
  482.9 57.0 %collective-permute-start.2 = (f32[2048,256]{0,1:T(8,128)S(1)}, f32[2048,256]{0,1:T(8,128)S(1)}, u32[]{:S(2)}, u32[]{:S(2)}) collective-permute-start(f32[2048,256]{0,1:T(8,128)S(1)} %add.103), channel_id=1, source_target_pairs={{0,8},{2,10},{4,12},{6,14},{8,0},{10,2},{12,4},{14,6},{16,24},{18,... | collective-permute-start | bytes 6291464 | tf_op jit(solution)/shard_map/ppermute | solution.py:13
  540.2 90.5 %collective-permute-start.3 = (f32[2048,256]{0,1:T(8,128)S(1)}, f32[2048,256]{0,1:T(8,128)}, u32[]{:S(2)}, u32[]{:S(2)}) collective-permute-start(f32[2048,256]{0,1:T(8,128)S(1)} %add.104), channel_id=1, source_target_pairs={{0,16},{2,18},{4,20},{6,22},{8,24},{10,26},{12,28},{14,30},{16,0},... | collective-permute-start | bytes 6291464 | tf_op jit(solution)/shard_map/ppermute | solution.py:13
  636.9 6.2 copy-start.1
Sparse Core Ops, SparseCore 0:
  290.8 13.2 reduce-scatter.2
  381.2 38.7 reduce-scatter.4
